TPU v7x, 256 devices: a whole 4x4x8 slice. The times are simulated.
256 devices in a mesh: sp: 32 (over z, x), tp: 8 (over y, core).
Axes of the slice: x: 4, y: 4, z: 8, core: 2. Of those that a mesh axis runs over, the one named last changes fastest.
Arguments:
- residual: bfloat16 [10240, 2048], P(('sp', 'tp')), may hold values from -6 to 6
- query_narrow: bfloat16 [10240, 1024], P('sp', 'tp'), may hold values from -48 to 48
- key_narrow: bfloat16 [10240, 1024], P('sp', 'tp'), may hold values from -48 to 48
- value_narrow: bfloat16 [10240, 1024], P('sp', 'tp'), may hold values from -6 to 6
- query_wide: bfloat16 [10240, 2048], P('sp', 'tp'), may hold values from -48 to 48
- key_wide: bfloat16 [10240, 2048], P('sp', 'tp'), may hold values from -48 to 48
- value_wide: bfloat16 [10240, 1024], P('sp', 'tp'), may hold values from -6 to 6
- subtract_narrow: float32 [8], P('tp'), may hold values from 0.3 to 0.8
- subtract_wide: float32 [8], P('tp'), may hold values from 0.3 to 0.8
- head_gain: float32 [128], replicated, may hold values from 0.1 to 1.9
- out_narrow: bfloat16 [1024, 2048], replicated, may hold values from -0.125 to 0.125
- out_wide: bfloat16 [1024, 2048], replicated, may hold values from -0.125 to 0.125
- norm1_gain: float32 [2048], replicated, may hold values from 0.1 to 1.9
- norm2_gain: float32 [2048], replicated, may hold values from 0.1 to 1.9
- expert_ids: int32 [10240, 2], P(('sp', 'tp')), may hold values from 0 to 31, all different within a row; in each aligned block of 40 rows (0 to 39, 40 to 79, ...) at most 3 rows name the same one
- expert_weight: float32 [10240, 2], P(('sp', 'tp')), may hold values from 0.1 to 1
- gate_proj: bfloat16 [32, 2048, 2048], P('sp', None, 'tp'), may hold values from -0.125 to 0.125
- up_proj: bfloat16 [32, 2048, 2048], P('sp', None, 'tp'), may hold values from -0.125 to 0.125
- down_proj: bfloat16 [32, 2048, 2048], P('sp', 'tp'), may hold values from -0.125 to 0.125
Outputs:
- layer_out: bfloat16 [10240, 2048], P(('sp', 'tp'))
Inputs may be any that keep to these rules, and one draw needn't show every extreme that they name: `expert_ids`: each row names 2 different experts. Among the 40 rows of one device no expert is named more than 3 times, and in some device's rows some expert is named exactly 3 times.
All inputs are finite; a program needn't handle non-finite values.
Results may differ from a plain program's by a relative error of at most 0.014.
Values may be sent and summed in bfloat16 or wider, within the bound.
A program may use at most 128 MiB of HBM per device.

v0:
```python
import jax
import jax.numpy as jnp
from jax import lax
from jax.sharding import PartitionSpec as P

residual_scale = 2.0**0.5


def in_one_piece(arrays, axis, dim, along):
    ends, at = ([], 0)
    for a in arrays[:-1]:
        at += a.shape[along]
        ends.append(at)
    both = jnp.concatenate(arrays, axis=along)
    return tuple(jnp.split(lax.all_gather(both, axis, axis=dim, tiled=True), ends, axis=along))


def in_blocks(value, dim, devices):
    before, after = (value.shape[:dim], value.shape[dim + 1 :])
    return jnp.moveaxis(value.reshape(*before, devices, -1, *after), dim, 0)


def sent_and_summed(value, axis, dim):
    devices = lax.axis_size(axis)
    pieces = lax.all_to_all(in_blocks(value, dim, devices), axis, 0, 0, tiled=True)
    return jnp.sum(pieces.astype(jnp.float32), axis=0)


def items_in_groups(value, axis, split_dim, concat_dim, work, item_dim, out_dim):
    items = jax.tree.leaves(value)[0].shape[item_dim]
    count = 2 if items % 2 == 0 else 1
    outs = []
    for k in range(count):
        group = jax.tree.map(
            lambda a: lax.slice_in_dim(
                a, k * (items // count), (k + 1) * (items // count), axis=item_dim
            ),
            value,
        )
        outs.append(
            work(
                lax.all_to_all(
                    group, axis, split_axis=split_dim, concat_axis=concat_dim, tiled=True
                )
            )
        )
    return jax.tree.map(lambda *parts: jnp.concatenate(parts, axis=out_dim), *outs)


def layer_norm(values, gain):
    center = jnp.mean(values, -1, keepdims=True)
    spread = jnp.mean(jnp.square(values - center), -1, keepdims=True)
    return (values - center) * lax.rsqrt(spread + 1e-05) * gain


def block_take(shards, shard_rows):
    take = shards
    for count in range(shards, 0, -1):
        if shards % count == 0 and count * shard_rows >= 512:
            take = count
    return take


def start_carry(head_count, tok_rows, value_size):
    return (
        jnp.full((head_count, 2, tok_rows), -1e30, jnp.float32),
        jnp.zeros((head_count, 2, tok_rows), jnp.float32),
        jnp.zeros((head_count, 2, tok_rows, value_size), jnp.float32),
    )


def absorb_keys(carry, queries, key_piece, value_piece, shard_rows):
    head_count = queries.shape[1]
    key_size = queries.shape[3]
    shards = key_piece.shape[0] // shard_rows
    take = block_take(shards, shard_rows)
    span = take * shard_rows

    def one_block(step_index, state):
        rowtop, total, summed = state
        key_block = lax.dynamic_slice_in_dim(key_piece, step_index * span, span, 0).reshape(
            span, head_count, 2, key_size
        )
        value_block = lax.dynamic_slice_in_dim(value_piece, step_index * span, span, 0).reshape(
            span, head_count, -1
        )
        scores = jnp.einsum(
            "qhmd,khmd->hmqk", queries, key_block, preferred_element_type=jnp.float32
        ) * key_size ** (-0.5)
        newtop = jnp.maximum(rowtop, jnp.max(scores, -1))
        shrink = jnp.exp(rowtop - newtop)
        expo = jnp.exp(scores - newtop[..., None])
        total = total * shrink + jnp.sum(expo, -1)
        summed = summed * shrink[..., None] + jnp.einsum(
            "hmqk,khe->hmqe",
            expo.astype(jnp.bfloat16),
            value_block,
            preferred_element_type=jnp.float32,
        )
        return (newtop, total, summed)

    return lax.fori_loop(0, shards // take, one_block, carry)


def finish_heads(carry, subtract, head_gain):
    rowtop, total, summed = carry
    mapped = summed / total[..., None]
    diff = mapped[:, 0] - subtract[:, None, None] * mapped[:, 1]
    normed = diff * lax.rsqrt(jnp.mean(diff * diff, -1, keepdims=True) + 1e-06) * head_gain
    return jnp.transpose(normed, (1, 0, 2)).reshape(diff.shape[1], -1).astype(jnp.bfloat16)


def on_device(
    residual,
    query_narrow,
    key_narrow,
    value_narrow,
    query_wide,
    key_wide,
    value_wide,
    subtract_narrow,
    subtract_wide,
    head_gain,
    out_narrow,
    out_wide,
    norm1_gain,
    norm2_gain,
    expert_ids,
    expert_weight,
    gate_proj,
    up_proj,
    down_proj,
):
    tok_rows = query_narrow.shape[0]
    head_count = subtract_narrow.shape[0]
    value_size = head_gain.shape[0]
    narrow_queries = query_narrow.reshape(tok_rows, head_count, 2, -1)
    wide_queries = query_wide.reshape(tok_rows, head_count, 2, -1)
    narrow_start = start_carry(head_count, tok_rows, value_size)
    wide_start = start_carry(head_count, tok_rows, value_size)
    pieces = in_one_piece((key_narrow, value_narrow), "sp", 0, 1)
    narrow_state = absorb_keys(narrow_start, narrow_queries, pieces[0], pieces[1], tok_rows)
    pieces = in_one_piece((key_wide, value_wide), "sp", 0, 1)
    wide_state = absorb_keys(wide_start, wide_queries, pieces[0], pieces[1], tok_rows)
    attended_narrow = finish_heads(narrow_state, subtract_narrow, head_gain)
    attended_wide = finish_heads(wide_state, subtract_wide, head_gain)
    offset = lax.axis_index("tp") * head_count * value_size
    local_narrow = lax.dynamic_slice_in_dim(out_narrow, offset, head_count * value_size, 0)
    local_wide = lax.dynamic_slice_in_dim(out_wide, offset, head_count * value_size, 0)
    mix = sent_and_summed(
        (
            jnp.dot(attended_narrow, local_narrow, preferred_element_type=jnp.float32)
            + jnp.dot(attended_wide, local_wide, preferred_element_type=jnp.float32)
        ).astype(jnp.bfloat16),
        "tp",
        0,
    )
    hidden = layer_norm(residual_scale * residual.astype(jnp.float32) + mix, norm1_gain).astype(
        jnp.bfloat16
    )
    local_rows, top_count = expert_ids.shape
    experts = lax.axis_size("sp")
    capacity = max(2, 3 * local_rows * top_count // (2 * experts))
    flat_ids = expert_ids.reshape(-1)
    onehot = (flat_ids[:, None] == jnp.arange(experts, dtype=jnp.int32)[None, :]).astype(jnp.int32)
    before = jnp.cumsum(onehot, 0) - onehot
    position = jnp.sum(before * onehot, 1)
    slots = (flat_ids * capacity + position).reshape(local_rows, top_count)
    dispatch_table = jnp.any(
        jnp.arange(experts * capacity, dtype=jnp.int32)[:, None, None] == slots[None], -1
    ).astype(jnp.bfloat16)
    outgoing = jnp.dot(dispatch_table, hidden, preferred_element_type=jnp.float32).astype(
        jnp.bfloat16
    )
    outgoing = outgoing.reshape(experts, capacity, -1)

    def run_expert(received):
        gathered = lax.all_gather(received, "tp", axis=1, tiled=True)
        flat_rows = gathered.reshape(-1, gathered.shape[2])
        gate_part = jnp.dot(flat_rows, gate_proj[0], preferred_element_type=jnp.float32)
        up_part = jnp.dot(flat_rows, up_proj[0], preferred_element_type=jnp.float32)
        inner = (jax.nn.silu(gate_part) * up_part).astype(jnp.bfloat16)
        partial_out = jnp.dot(inner, down_proj[0], preferred_element_type=jnp.float32).reshape(
            gathered.shape
        )
        summed = lax.psum_scatter(
            partial_out.astype(jnp.bfloat16), "tp", scatter_dimension=1, tiled=True
        )
        return lax.all_to_all(summed, "sp", split_axis=0, concat_axis=0, tiled=True)

    returned = items_in_groups(outgoing, "sp", 0, 0, run_expert, 1, 1)
    returned_flat = returned.reshape(experts * capacity, -1)
    picked = returned_flat[slots].astype(jnp.float32)
    routed = jnp.sum(expert_weight[..., None] * picked, 1)
    return layer_norm(residual_scale * hidden.astype(jnp.float32) + routed, norm2_gain).astype(
        jnp.bfloat16
    )


def solution(mesh):
    placed = (
        P(("sp", "tp"), None),
        P("sp", "tp"),
        P("sp", "tp"),
        P("sp", "tp"),
        P("sp", "tp"),
        P("sp", "tp"),
        P("sp", "tp"),
        P("tp"),
        P("tp"),
        P(),
        P(),
        P(),
        P(),
        P(),
        P(("sp", "tp"), None),
        P(("sp", "tp"), None),
        P("sp", None, "tp"),
        P("sp", None, "tp"),
        P("sp", "tp", None),
    )
    return jax.shard_map(
        on_device, mesh=mesh, in_specs=placed, out_specs=P(("sp", "tp"), None), check_vma=False
    )
```

profile of v0, /device:TPU:25, one launch (start us, length us, event | category | flops | bytes accessed | tf_op | source)
XLA Modules:
  0.0 422.1 jit_solution(8756736317949425885)
XLA Ops:
  6.5 1.7 pad_maximum_fusion.1
  8.3 1.7 pad_maximum_fusion
  10.1 1.6 copy.88
  14.7 79.7 %all-gather.4.cloned.1.call-done = bf16[10240,256]{1,0:T(8,128)(2,1)} async-done(((bf16[320,256]{1,0:T(8,128)(2,1)}), bf16[10240,256]{1,0:T(8,128)(2,1)}) %all-gather.4.cloned.1.call-update) | async-done | bytes 5242896 | tf_op jit(solution)/shard_map/all_gather | solution.py:15
  94.4 4.1 fusion.57
  98.5 72.0 %while.36 = (s32[]{:T(128)}, f32[1,2,320]{2,1,0:T(2,128)S(1)}, f32[1,2,320]{2,1,0:T(2,128)S(1)}, f32[1,2,320,128]{3,2,1,0:T(8,128)S(1)}, bf16[10240,128]{1,0:T(8...) while((s32[]{:T(128)}, f32[1,2,320]{2,1,0:T(2,128)S(1)}, ...), condition=%wide.region_3.0_spmd.clone, body=%wide.region_0.0_spmd.clone.sunk | while | flops 160812800 | bytes 6676655 | solution.py:102
  101.1 1.5 fusion.82
  114.5 1.5 fusion.82
  119.0 1.5 fusion.82
  128.0 1.5 fusion.82
  132.5 1.5 fusion.82
  141.5 1.4 fusion.82
  159.5 1.5 fusion.82
  164.0 1.5 fusion.82
  168.5 1.4 fusion.82
  170.8 3.1 fusion.35
  173.9 17.8 %all-gather.6.cloned.1.call-done = bf16[10240,384]{1,0:T(8,128)(2,1)} async-done(((bf16[320,384]{1,0:T(8,128)(2,1)}), bf16[10240,384]{1,0:T(8,128)(2,1)}) %all-gather.6.cloned.1.call-update) | async-done | bytes 7864336 | tf_op jit(solution)/shard_map/all_gather | solution.py:15
  191.6 4.2 split.18
  195.8 2.9 split.19
  198.8 58.4 %while.37 = (s32[]{:T(128)}, f32[1,2,320]{2,1,0:T(2,128)S(1)}, f32[1,2,320]{2,1,0:T(2,128)S(1)}, f32[1,2,320,128]{3,2,1,0:T(8,128)S(1)}, bf16[10240,256]{1,0:T(8...) while((s32[]{:T(128)}, f32[1,2,320]{2,1,0:T(2,128)S(1)}, ...), condition=%wide.region_8.0_spmd.clone, body=%wide.region_5.8_spmd.clone.sunk | while | flops 213241600 | bytes 7577775 | solution.py:102
  257.5 3.5 fusion.28
  261.0 6.1 %all-to-all-start = ((bf16[8,40,2048]{2,1,0:T(8,128)(2,1)}), bf16[8,40,2048]{2,1,0:T(8,128)(2,1)S(1)}, u32[]{:S(2)}, u32[]{:S(2)}) async-start(bf16[8,40,2048]{2,1,0:T(8,128)(2,1)} %bitcast.7), calls=%async_computation | async-start | bytes 2621440 | tf_op jit(solution)/shard_map/all_to_all | solution.py:25
  268.0 15.2 %all-to-all-done = bf16[8,40,2048]{2,1,0:T(8,128)(2,1)S(1)} async-done(((bf16[8,40,2048]{2,1,0:T(8,128)(2,1)}), bf16[8,40,2048]{2,1,0:T(8,128)(2,1)S(1)}, u32[]{:S(2)}, u32[]{:S(2)}) %all-to-all-start) | async-done | bytes 1310752 | tf_op jit(solution)/shard_map/all_to_all | solution.py:25
  284.4 20.4 %all_to_all.15 = bf16[32,3,2048]{2,1,0:T(4,128)(2,1)S(1)} all-to-all(bf16[32,3,2048]{2,1,0:T(4,128)(2,1)S(1)} %reshape.302), channel_id=1, replica_groups=mesh['sp'=32,'tp'=8] {'sp'}, dimensions={0} | all-to-all | bytes 786432 | tf_op jit(solution)/shard_map/all_to_all | solution.py:42
  306.1 28.0 %all-gather.8.cloned.1.call-done = bf16[32,24,2048]{2,0,1:T(8,128)(2,1)} async-done(((bf16[32,3,2048]{2,0,1:T(8,128)(2,1)}), bf16[32,24,2048]{2,0,1:T(8,128)(2,1)}) %all-gather.8.cloned.1.call-update) | async-done | bytes 3145744 | tf_op jit(solution)/shard_map/all_gather | solution.py:178
  334.1 3.6 copy.96
  337.8 2.3 fusion.32
  342.1 3.4 copy.97
  345.5 37.9 %reduce-scatter.2.cloned.1.call-done = bf16[32,3,2048]{2,0,1:T(8,128)(2,1)} async-done(((bf16[32,24,2048]{2,0,1:T(8,128)(2,1)}), bf16[32,3,2048]{2,0,1:T(8,128)(2,1)}) %reduce-scatter.2.cloned.1.call-update) | async-done | bytes 393232 | tf_op jit(solution)/shard_map/reduce_scatter | solution.py:186
  383.4 2.1 copy.98
  385.5 9.2 %all-to-all-start.2 = ((bf16[32,3,2048]{2,1,0:T(4,128)(2,1)}), bf16[32,3,2048]{2,1,0:T(4,128)(2,1)S(1)}, u32[]{:S(2)}, u32[]{:S(2)}) async-start(bf16[32,3,2048]{2,1,0:T(4,128)(2,1)} %copy.98), calls=%async_computation.3 | async-start | bytes 1048576 | tf_op jit(solution)/shard_map/all_to_all | solution.py:189
  395.0 16.9 %all-to-all-done.2 = bf16[32,3,2048]{2,1,0:T(4,128)(2,1)S(1)} async-done(((bf16[32,3,2048]{2,1,0:T(4,128)(2,1)}), bf16[32,3,2048]{2,1,0:T(4,128)(2,1)S(1)}, u32[]{:S(2)}, u32[]{:S(2)}) %all-to-all-start.2) | async-done | bytes 393248 | tf_op jit(solution)/shard_map/all_to_all | solution.py:189
  (320 shorter events, 127.2 us)
Async XLA Ops:
  6.5 334.5 %copy-start = (bf16[1,256,2048]{2,1,0:T(8,128)(2,1)S(1)}, bf16[1,256,2048]{2,1,0:T(8,128)(2,1)}, u32[]{:S(2)}) copy-start(bf16[1,256,2048]{2,1,0:T(8,128)(2,1)} %param.41) | copy-start | bytes 3145732
  6.5 87.8 %all-gather.4.cloned.1.call-start = ((), (), s32[]{:S(2)}) async-start(), calls=%async_computation.4 | async-start | bytes 5406720 | tf_op jit(solution)/shard_map/all_gather | solution.py:15
  8.3 183.4 %all-gather.6.cloned.1.call-start = ((), (), s32[]{:S(2)}) async-start(), calls=%async_computation.5 | async-start | bytes 8110080 | tf_op jit(solution)/shard_map/all_gather | solution.py:15
  98.5 72.3 %copy-start.6 = (f32[128]{0:T(128)S(1)}, f32[128]{0:T(128)}, u32[]{:S(2)}) copy-start(f32[128]{0:T(128)} %param.32) | copy-start | bytes 1540
  195.8 2.9 copy-start.1
  257.5 9.6 %copy-start.5 = (s32[40,2]{0,1:T(2,128)S(1)}, s32[40,2]{0,1:T(2,128)}, u32[]{:S(2)}) copy-start(s32[40,2]{0,1:T(2,128)} %param.37) | copy-start | bytes 964
  261.0 22.4 %copy-start.2 = (bf16[40,2048]{1,0:T(8,128)(2,1)S(1)}, bf16[40,2048]{1,0:T(8,128)(2,1)}, u32[]{:S(2)}) copy-start(bf16[40,2048]{1,0:T(8,128)(2,1)} %param.23) | copy-start | bytes 491524
  261.0 22.7 %copy-start.3 = (f32[2048]{0:T(1024)S(1)}, f32[2048]{0:T(1024)}, u32[]{:S(2)}) copy-start(f32[2048]{0:T(1024)} %param.35) | copy-start | bytes 24580
  261.0 22.2 %all-to-all-start = ((bf16[8,40,2048]{2,1,0:T(8,128)(2,1)}), bf16[8,40,2048]{2,1,0:T(8,128)(2,1)S(1)}, u32[]{:S(2)}, u32[]{:S(2)}) async-start(bf16[8,40,2048]{2,1,0:T(8,128)(2,1)} %bitcast.7), calls=%async_computation | async-start | bytes 2621440 | tf_op jit(solution)/shard_map/all_to_all | solution.py:25
  267.1 67.1 %all-gather.8.cloned.1.call-start = ((), (), s32[]{:S(2)}) async-start(), calls=%async_computation.6 | async-start | bytes 3538944 | tf_op jit(solution)/shard_map/all_gather | solution.py:178
  305.9 77.5 %reduce-scatter.2.cloned.1.call-start = ((), (), s32[]{:S(2)}) async-start(), calls=%async_computation.7 | async-start | bytes 3538944 | tf_op jit(solution)/shard_map/reduce_scatter | solution.py:186
  337.7 2.3 copy-start.8
  345.5 49.5 %copy-start.7 = (f32[40,2]{0,1:T(2,128)S(1)}, f32[40,2]{0,1:T(2,128)}, u32[]{:S(2)}) copy-start(f32[40,2]{0,1:T(2,128)} %param.38) | copy-start | bytes 964
  385.5 26.4 %all-to-all-start.2 = ((bf16[32,3,2048]{2,1,0:T(4,128)(2,1)}), bf16[32,3,2048]{2,1,0:T(4,128)(2,1)S(1)}, u32[]{:S(2)}, u32[]{:S(2)}) async-start(bf16[32,3,2048]{2,1,0:T(4,128)(2,1)} %copy.98), calls=%async_computation.3 | async-start | bytes 1048576 | tf_op jit(solution)/shard_map/all_to_all | solution.py:189
  412.2 2.6 copy-start.4
Sparse Core Ops, SparseCore 0:
  9.9 84.4 all-gather.3
  97.0 94.6 all-gather.5
  306.0 28.0 all-gather.7
  345.6 37.7 reduce-scatter.1
where the time goes:
time: 425 us; the launch traced here: 422 us
  waiting for transfers between devices  195 us (46%)
  matrix products  87.6 us (21%)
  local copies, waits for them, and re-layouts  64.1 us (15%)
  other arithmetic  22.6 us (5%)
  blocking collectives  20.4 us (5%)
  starting transfers between devices  15.5 us (4%)
  between operations  14.7 us (3%)
    all_gather x2, waiting for transfers between devices, in_one_piece(): lax.all_gather(both, axis, axis=dim, tiled=True)  97.4 us
    dot_general x32, matrix products, one_block(): jnp.einsum('hmqk,khe->hmqe', expo.astype(jnp.bfloat16), value_block, pref...  46.3 us
    reduce_scatter x1, waiting for transfers between devices, run_expert(): lax.psum_scatter(partial_out.astype(jnp.bfloat16), 'tp', scatter_dimensio...  37.9 us
    dynamic_slice x64, local copies, waits for them, and re-layouts, one_block(): lax.dynamic_slice_in_dim(key_piece, step_index * span, span, 0)  36.8 us
    dot_general x32, matrix products, one_block(): jnp.einsum('qhmd,khmd->hmqk', queries, key_block, preferred_element_type=...  30.2 us
    all_gather x1, waiting for transfers between devices, run_expert(): gathered = lax.all_gather(received, 'tp', axis=1, tiled=True)  28 us
    all_to_all x1, blocking collectives, items_in_groups(): lax.all_to_all(group, axis, split_axis=split_dim, concat_axis=concat_dim,...  20.4 us
    all_to_all x1, waiting for transfers between devices, run_expert(): return lax.all_to_all(summed, 'sp', split_axis=0, concat_axis=0, tiled=True)  16.9 us
  transfers between devices with their start and end apart: 6, of which 6 were waited for; matrix products, arithmetic and copies ran while one was open for 20% of the time, Pallas kernels for 0%

commit v1 on v0

--- a/solution.py
+++ b/solution.py
@@ -1,9 +1,26 @@
+import functools
 import jax
 import jax.numpy as jnp
 from jax import lax
 from jax.sharding import PartitionSpec as P
 
 residual_scale = 2.0**0.5
+
+
+def form_inputs(z, dim_no):
+    u1 = jnp.concatenate(
+        jax.lax.all_to_all(
+            jnp.stack(tuple((z for _ in range(jax.lax.psum(1, axis_name="tp"))))),
+            axis_name="tp",
+            split_axis=0,
+            concat_axis=0,
+        ),
+        axis=dim_no,
+    )
+    return u1
+
+
+shape_surface_up = functools.partial(form_inputs, dim_no=1)
 
 
 def in_one_piece(arrays, axis, dim, along):
@@ -175,7 +192,7 @@
     outgoing = outgoing.reshape(experts, capacity, -1)
 
     def run_expert(received):
-        gathered = lax.all_gather(received, "tp", axis=1, tiled=True)
+        gathered = shape_surface_up(received)
         flat_rows = gathered.reshape(-1, gathered.shape[2])
         gate_part = jnp.dot(flat_rows, gate_proj[0], preferred_element_type=jnp.float32)
         up_part = jnp.dot(flat_rows, up_proj[0], preferred_element_type=jnp.float32)

time: 425 us -> 446 us (1.049)
  blocking collectives: 20.4 us -> 63.6 us
  waiting for transfers between devices: 195 us -> 163 us
  local copies, waits for them, and re-layouts: 64.1 us -> 73.7 us
    all_to_all x0 -> x1, blocking collectives: none -> 43.2 us  [form_inputs(): jax.lax.all_to_all(jnp.stack(tuple((z for _ in range(jax.lax.psum(1, axis...]
    all_gather x1 -> x0, waiting for transfers between devices: 28 us -> none  [run_expert(): gathered = lax.all_gather(received, 'tp', axis=1, tiled=True)]
    another operation x0 -> x2, local copies, waits for them, and re-layouts: none -> 9.19 us  [the longest x1 8.81 us: run_expert(): flat_rows = gathered.reshape(-1, gathered.shape[2])]
    reshape x0 -> x1, local copies, waits for them, and re-layouts: none -> 4.63 us  [form_inputs(): jnp.concatenate(jax.lax.all_to_all(jnp.stack(tuple((z for _ in range(jax....]
  transfers between devices with their start and end apart: 6 -> 5, of which waited for: 6 -> 5; matrix products, arithmetic and copies ran while one was open for 20% -> 19% of each run, Pallas kernels for 0% -> 0%
where the time goes in v1:
time: 446 us; the launch traced here: 443 us
  waiting for transfers between devices  163 us (37%)
  matrix products  88.7 us (20%)
  local copies, waits for them, and re-layouts  73.7 us (17%)
  blocking collectives  63.6 us (14%)
  other arithmetic  22.6 us (5%)
  starting transfers between devices  15.3 us (3%)
  between operations  14.7 us (3%)
    all_gather x2, waiting for transfers between devices, in_one_piece(): lax.all_gather(both, axis, axis=dim, tiled=True)  97.4 us
    dot_general x32, matrix products, one_block(): jnp.einsum('hmqk,khe->hmqe', expo.astype(jnp.bfloat16), value_block, pref...  46.3 us
    all_to_all x1, blocking collectives, form_inputs(): jax.lax.all_to_all(jnp.stack(tuple((z for _ in range(jax.lax.psum(1, axis...  43.2 us
    dynamic_slice x64, local copies, waits for them, and re-layouts, one_block(): lax.dynamic_slice_in_dim(key_piece, step_index * span, span, 0)  36.8 us
    reduce_scatter x1, waiting for transfers between devices, run_expert(): lax.psum_scatter(partial_out.astype(jnp.bfloat16), 'tp', scatter_dimensio...  33.5 us
    dot_general x32, matrix products, one_block(): jnp.einsum('qhmd,khmd->hmqk', queries, key_block, preferred_element_type=...  30.2 us
    all_to_all x1, blocking collectives, items_in_groups(): lax.all_to_all(group, axis, split_axis=split_dim, concat_axis=concat_dim,...  20.4 us
    all_to_all x1, waiting for transfers between devices, run_expert(): return lax.all_to_all(summed, 'sp', split_axis=0, concat_axis=0, tiled=True)  16.9 us
  transfers between devices with their start and end apart: 5, of which 5 were waited for; matrix products, arithmetic and copies ran while one was open for 19% of the time, Pallas kernels for 0%

profile of v1, /device:TPU:25, one launch (start us, length us, event | category | flops | bytes accessed | tf_op | source)
XLA Modules:
  0.0 443.2 jit_solution(13553304272063400973)
XLA Ops:
  6.5 1.7 pad_maximum_fusion.1
  8.3 1.7 pad_maximum_fusion
  10.1 1.6 copy.76
  14.7 79.7 %all-gather.3.cloned.1.call-done = bf16[10240,256]{1,0:T(8,128)(2,1)} async-done(((bf16[320,256]{1,0:T(8,128)(2,1)}), bf16[10240,256]{1,0:T(8,128)(2,1)}) %all-gather.3.cloned.1.call-update) | async-done | bytes 5242896 | tf_op jit(solution)/shard_map/all_gather | solution.py:32
  94.4 4.1 fusion.57
  98.5 72.0 %while.36 = (s32[]{:T(128)}, f32[1,2,320]{2,1,0:T(2,128)S(1)}, f32[1,2,320]{2,1,0:T(2,128)S(1)}, f32[1,2,320,128]{3,2,1,0:T(8,128)S(1)}, bf16[10240,128]{1,0:T(8...) while((s32[]{:T(128)}, f32[1,2,320]{2,1,0:T(2,128)S(1)}, ...), condition=%wide.region_3.0_spmd.clone, body=%wide.region_0.0_spmd.clone.sunk | while | flops 160812800 | bytes 6676655 | solution.py:119
  101.1 1.5 fusion.82
  114.5 1.5 fusion.82
  119.0 1.5 fusion.82
  128.0 1.5 fusion.82
  132.5 1.5 fusion.82
  159.5 1.5 fusion.82
  164.0 1.5 fusion.82
  168.5 1.4 fusion.82
  170.8 3.1 fusion.35
  173.9 17.8 %all-gather.5.cloned.1.call-done = bf16[10240,384]{1,0:T(8,128)(2,1)} async-done(((bf16[320,384]{1,0:T(8,128)(2,1)}), bf16[10240,384]{1,0:T(8,128)(2,1)}) %all-gather.5.cloned.1.call-update) | async-done | bytes 7864336 | tf_op jit(solution)/shard_map/all_gather | solution.py:32
  191.6 4.2 split.18
  195.8 2.9 split.19
  198.8 58.4 %while.37 = (s32[]{:T(128)}, f32[1,2,320]{2,1,0:T(2,128)S(1)}, f32[1,2,320]{2,1,0:T(2,128)S(1)}, f32[1,2,320,128]{3,2,1,0:T(8,128)S(1)}, bf16[10240,256]{1,0:T(8...) while((s32[]{:T(128)}, f32[1,2,320]{2,1,0:T(2,128)S(1)}, ...), condition=%wide.region_8.0_spmd.clone, body=%wide.region_5.8_spmd.clone.sunk | while | flops 213241600 | bytes 7577775 | solution.py:119
  257.5 3.5 fusion.28
  261.0 6.1 %all-to-all-start = ((bf16[8,40,2048]{2,1,0:T(8,128)(2,1)}), bf16[8,40,2048]{2,1,0:T(8,128)(2,1)S(1)}, u32[]{:S(2)}, u32[]{:S(2)}) async-start(bf16[8,40,2048]{2,1,0:T(8,128)(2,1)} %bitcast.7), calls=%async_computation | async-start | bytes 2621440 | tf_op jit(solution)/shard_map/all_to_all | solution.py:42
  268.0 15.2 %all-to-all-done = bf16[8,40,2048]{2,1,0:T(8,128)(2,1)S(1)} async-done(((bf16[8,40,2048]{2,1,0:T(8,128)(2,1)}), bf16[8,40,2048]{2,1,0:T(8,128)(2,1)S(1)}, u32[]{:S(2)}, u32[]{:S(2)}) %all-to-all-start) | async-done | bytes 1310752 | tf_op jit(solution)/shard_map/all_to_all | solution.py:42
  284.4 20.4 %all_to_all.20 = bf16[32,3,2048]{2,1,0:T(4,128)(2,1)S(1)} all-to-all(bf16[32,3,2048]{2,1,0:T(4,128)(2,1)S(1)} %reshape.304), channel_id=1, replica_groups=mesh['sp'=32,'tp'=8] {'sp'}, dimensions={0} | all-to-all | bytes 786432 | tf_op jit(solution)/shard_map/all_to_all | solution.py:59
  305.5 43.2 %all_to_all.21 = bf16[8,32,3,2048]{3,1,2,0:T(8,128)(2,1)S(1)} all-to-all(bf16[8,32,3,2048]{3,1,2,0:T(8,128)(2,1)S(1)} %stack.2), channel_id=1, replica_groups=mesh['sp'=32,'tp'=8] {'tp'}, dimensions={0} | all-to-all | bytes 6291456 | tf_op jit(solution)/shard_map/all_to_all | solution.py:12
  348.7 4.6 %copy.84 = bf16[32,8,3,2048]{3,2,1,0:T(4,128)(2,1)} copy(bf16[32,8,3,2048]{3,0,2,1:T(8,128)(2,1)S(1)} %bitcast.151) | data formatting | bytes 6291456 | tf_op jit(solution)/shard_map/reshape | solution.py:11
  353.3 8.8 %reshape_reshape.3 = bf16[768,2048]{1,0:T(8,128)(2,1)} reshape(bf16[32,8,3,2048]{3,2,1,0:T(4,128)(2,1)} %copy.84) | data formatting | bytes 6291456 | tf_op jit(solution)/shard_map/reshape;reshape | solution.py:196
  362.1 3.3 fusion.32
  367.6 3.4 copy.85
  371.0 33.5 %reduce-scatter.2.cloned.1.call-done = bf16[32,3,2048]{2,0,1:T(8,128)(2,1)} async-done(((bf16[32,24,2048]{2,0,1:T(8,128)(2,1)}), bf16[32,3,2048]{2,0,1:T(8,128)(2,1)}) %reduce-scatter.2.cloned.1.call-update) | async-done | bytes 393232 | tf_op jit(solution)/shard_map/reduce_scatter | solution.py:203
  404.5 2.1 copy.86
  406.6 9.2 %all-to-all-start.3 = ((bf16[32,3,2048]{2,1,0:T(4,128)(2,1)}), bf16[32,3,2048]{2,1,0:T(4,128)(2,1)S(1)}, u32[]{:S(2)}, u32[]{:S(2)}) async-start(bf16[32,3,2048]{2,1,0:T(4,128)(2,1)} %copy.86), calls=%async_computation.4 | async-start | bytes 1048576 | tf_op jit(solution)/shard_map/all_to_all | solution.py:206
  416.1 16.9 %all-to-all-done.3 = bf16[32,3,2048]{2,1,0:T(4,128)(2,1)S(1)} async-done(((bf16[32,3,2048]{2,1,0:T(4,128)(2,1)}), bf16[32,3,2048]{2,1,0:T(4,128)(2,1)S(1)}, u32[]{:S(2)}, u32[]{:S(2)}) %all-to-all-start.3) | async-done | bytes 393248 | tf_op jit(solution)/shard_map/all_to_all | solution.py:206
  (322 shorter events, 128.2 us)
Async XLA Ops:
  6.5 360.0 %copy-start = (bf16[1,256,2048]{2,1,0:T(8,128)(2,1)S(1)}, bf16[1,256,2048]{2,1,0:T(8,128)(2,1)}, u32[]{:S(2)}) copy-start(bf16[1,256,2048]{2,1,0:T(8,128)(2,1)} %param.41) | copy-start | bytes 3145732
  6.5 87.8 %all-gather.3.cloned.1.call-start = ((), (), s32[]{:S(2)}) async-start(), calls=%async_computation.5 | async-start | bytes 5406720 | tf_op jit(solution)/shard_map/all_gather | solution.py:32
  8.3 183.4 %all-gather.5.cloned.1.call-start = ((), (), s32[]{:S(2)}) async-start(), calls=%async_computation.6 | async-start | bytes 8110080 | tf_op jit(solution)/shard_map/all_gather | solution.py:32
  98.5 72.3 %copy-start.7 = (f32[128]{0:T(128)S(1)}, f32[128]{0:T(128)}, u32[]{:S(2)}) copy-start(f32[128]{0:T(128)} %param.32) | copy-start | bytes 1540
  195.8 2.9 copy-start.1
  257.5 9.6 %copy-start.6 = (s32[40,2]{0,1:T(2,128)S(1)}, s32[40,2]{0,1:T(2,128)}, u32[]{:S(2)}) copy-start(s32[40,2]{0,1:T(2,128)} %param.37) | copy-start | bytes 964
  261.0 22.4 %copy-start.3 = (bf16[40,2048]{1,0:T(8,128)(2,1)S(1)}, bf16[40,2048]{1,0:T(8,128)(2,1)}, u32[]{:S(2)}) copy-start(bf16[40,2048]{1,0:T(8,128)(2,1)} %param.23) | copy-start | bytes 491524
  261.0 22.7 %copy-start.4 = (f32[2048]{0:T(1024)S(1)}, f32[2048]{0:T(1024)}, u32[]{:S(2)}) copy-start(f32[2048]{0:T(1024)} %param.35) | copy-start | bytes 24580
  261.0 22.2 %all-to-all-start = ((bf16[8,40,2048]{2,1,0:T(8,128)(2,1)}), bf16[8,40,2048]{2,1,0:T(8,128)(2,1)S(1)}, u32[]{:S(2)}, u32[]{:S(2)}) async-start(bf16[8,40,2048]{2,1,0:T(8,128)(2,1)} %bitcast.7), calls=%async_computation | async-start | bytes 2621440 | tf_op jit(solution)/shard_map/all_to_all | solution.py:42
  267.1 137.4 %reduce-scatter.2.cloned.1.call-start = ((), (), s32[]{:S(2)}) async-start(), calls=%async_computation.7 | async-start | bytes 3538944 | tf_op jit(solution)/shard_map/reduce_scatter | solution.py:203
  362.1 3.3 copy-start.2
  362.1 3.4 copy-start.9
  371.0 45.0 %copy-start.8 = (f32[40,2]{0,1:T(2,128)S(1)}, f32[40,2]{0,1:T(2,128)}, u32[]{:S(2)}) copy-start(f32[40,2]{0,1:T(2,128)} %param.38) | copy-start | bytes 964
  406.6 26.4 %all-to-all-start.3 = ((bf16[32,3,2048]{2,1,0:T(4,128)(2,1)}), bf16[32,3,2048]{2,1,0:T(4,128)(2,1)S(1)}, u32[]{:S(2)}, u32[]{:S(2)}) async-start(bf16[32,3,2048]{2,1,0:T(4,128)(2,1)} %copy.86), calls=%async_computation.4 | async-start | bytes 1048576 | tf_op jit(solution)/shard_map/all_to_all | solution.py:206
  433.3 2.6 copy-start.5
Sparse Core Ops, SparseCore 0:
  9.9 84.4 all-gather.2
  97.0 94.6 all-gather.4
  371.1 33.3 reduce-scatter.1
